TPU v7x, 32 devices: a whole 2x2x4 slice. The times are simulated.
32 devices in a mesh: sp: 4 (over x, core), tp: 8 (over z, y).
Axes of the slice: x: 2, y: 2, z: 4, core: 2. Of those that a mesh axis runs over, the one named last changes fastest.
Arguments:
- latent: bfloat16 [512, 4096], P('sp', 'tp'), may hold values from -60 to 60
- context: bfloat16 [64, 4096], P('sp', 'tp'), may hold values from -6 to 6
- conditioning: bfloat16 [4096], P('sp'), may hold values from -6 to 6
- context_prompt_vector: bfloat16 [4096], P('sp'), may hold values from -6 to 6
- shift_matrix: bfloat16 [4096, 4096], P('tp', 'sp'), may hold values from -0.09375 to 0.09375
- scale_matrix: bfloat16 [4096, 4096], P('tp', 'sp'), may hold values from -0.09375 to 0.09375
- residual_gate_matrix: bfloat16 [4096, 4096], P('tp', 'sp'), may hold values from -0.09375 to 0.09375
- query_matrix: bfloat16 [2048, 4096], P('tp'), may hold values from -0.09375 to 0.09375
- key_matrix: bfloat16 [2048, 4096], P('tp'), may hold values from -0.09375 to 0.09375
- value_matrix: bfloat16 [4096, 4096], P('tp'), may hold values from -0.09375 to 0.09375
- gate_matrix: bfloat16 [4096, 4096], P('tp'), may hold values from -0.09375 to 0.09375
- decay_down_factor: bfloat16 [2, 4096, 16], replicated, may hold values from -0.09375 to 0.09375
- decay_up_factor: bfloat16 [2, 16, 2048], replicated, may hold values from -1.5 to 1.5
- decay_key_bias: float32 [2, 2048], replicated, may hold values from -0.5 to 7
- spike_log_decay: float32 [2, 512, 16], P(None, 'sp'), may hold values from -2.8 to 0
- output_gain: float32 [4096], P('tp'), may hold values from 0.1 to 1.9
- output_matrix: bfloat16 [4096, 4096], P('tp'), may hold values from -0.375 to 0.375
Outputs:
- mixed: bfloat16 [512, 4096], P('sp', 'tp')
All inputs are finite; a program needn't handle non-finite values.
Results may differ from a plain program's by a relative error of at most 0.013.
Values may be sent and summed in bfloat16 or wider, within the bound.
A program may use at most 64 MiB of HBM per device.

v0:
```python
import jax
import jax.numpy as jnp
from jax import lax
from jax.sharding import PartitionSpec as P

D = 4096
HEADS = 16
DK = 128
DECAY_RANK = 16
BLK = 64
VGROUP = 64
epsilon = 1e-05
gate_norm = 16.0
precise = lax.Precision.HIGHEST


def for_sending(value):

    def short(part):
        return part.astype(jnp.bfloat16) if part.dtype == jnp.float32 else part

    return jax.tree.map(short, value)


def from_partner(value, axis, distance):
    return lax.ppermute(value, axis, [(i, i ^ 1 << distance) for i in range(lax.axis_size(axis))])


def carried_in(value, axis, combine, identity, reverse):
    peers, index = (lax.axis_size(axis), lax.axis_index(axis))
    everything = jax.tree.map(
        lambda part, kind: lax.all_gather(part.astype(kind), axis),
        value,
        (jnp.bfloat16, jnp.bfloat16),
    )
    start = jax.tree.map(
        lambda part, zero: jnp.broadcast_to(jnp.asarray(zero, part.dtype), part.shape),
        value,
        identity,
    )

    def turn(k, before):
        at = peers - 1 - k if reverse else k
        reached = at > index if reverse else at < index
        new = combine(
            before, jax.tree.map(lambda part, own: part[at].astype(own.dtype), everything, value)
        )
        return jax.tree.map(lambda a, b: jnp.where(reached, a, b), new, before)

    return lax.fori_loop(0, peers, turn, start)


def linear(rows, weight):
    return lax.dot_general(
        rows, weight, (((1,), (1,)), ((), ())), preferred_element_type=jnp.float32
    )


def modulated(rows, row_sum, row_squares, shift_vec, scale_vec):
    rows_f = rows.astype(jnp.float32)
    mean_val = row_sum / D
    variance = row_squares / D - mean_val * mean_val
    return (
        (rows_f - mean_val) * lax.rsqrt(variance + epsilon) * (1.0 + scale_vec) + shift_vec
    ).astype(jnp.bfloat16)


def reverse_rows(array):
    return jnp.flip(array, axis=0)


def end_state(key_rows, value_rows, log_decay):
    cumulative = jnp.cumsum(log_decay, axis=0)
    totals = cumulative[-1]
    weighted = key_rows * jnp.exp(totals - cumulative)
    return (jnp.exp(totals), jnp.einsum("nhd,nhe->hde", weighted, value_rows, precision=precise))


def combine(earlier, later):
    return (earlier[0] * later[0], later[0][..., None] * earlier[1] + later[1])


def blockwise(queries, key_rows, value_rows, log_decay, carried, block_len):
    length, head_count, _ = queries.shape
    value_width = value_rows.shape[-1]
    blocks = length // block_len

    def shaped(array):
        return array.reshape(blocks, block_len, head_count, array.shape[-1])

    triangle = jnp.tril(jnp.ones((block_len, block_len), jnp.float32))

    def advance(state_now, inputs):
        block_q, block_k, block_v, block_a = inputs
        cumulative = jnp.cumsum(block_a, axis=0)
        block_end = cumulative[-1]
        query_dec = block_q * jnp.exp(cumulative)
        scores = (
            jnp.einsum("ihd,jhd->hij", query_dec, block_k * jnp.exp(-cumulative), precision=precise)
            * triangle
        )
        result = jnp.einsum("hij,jhe->ihe", scores, block_v, precision=precise)
        result = result + jnp.einsum("ihd,hde->ihe", query_dec, state_now, precision=precise)
        state_next = state_now * jnp.exp(block_end)[:, :, None] + jnp.einsum(
            "jhd,jhe->hde", block_k * jnp.exp(block_end - cumulative), block_v, precision=precise
        )
        return (state_next, result)

    _, outputs = lax.scan(
        advance, carried, (shaped(queries), shaped(key_rows), shaped(value_rows), shaped(log_decay))
    )
    return outputs.reshape(length, head_count, value_width)


def head_channels(pieces, per_head, tp_index):
    for bit_number in range(per_head.bit_length() - 1):
        partner = from_partner(
            (for_sending(pieces[0]), for_sending(pieces[1]), for_sending(pieces[2])),
            "tp",
            bit_number,
        )
        upper = tp_index // (1 << bit_number) % 2 == 1
        pieces = tuple(
            (
                jnp.where(
                    upper,
                    jnp.concatenate([theirs, mine], axis=1),
                    jnp.concatenate([mine, theirs], axis=1),
                )
                for mine, theirs in zip(pieces, partner)
            )
        )
    return pieces


def context_totals(fwd_growth, fwd_state, bwd_growth, bwd_state, identity):

    def absorb(carried, piece):
        return (combine(carried, piece), None)

    total_fwd, _ = lax.scan(absorb, identity, (fwd_growth, fwd_state))
    total_bwd, _ = lax.scan(absorb, identity, (bwd_growth, bwd_state), reverse=True)
    return (total_fwd, total_bwd)


def stored(array):
    return lax.optimization_barrier(array.astype(jnp.bfloat16))


def local(
    latent,
    context,
    conditioning,
    context_prompt_vector,
    shift_matrix,
    scale_matrix,
    residual_gate_matrix,
    query_matrix,
    key_matrix,
    value_matrix,
    gate_matrix,
    decay_down_factor,
    decay_up_factor,
    decay_key_bias,
    spike_log_decay,
    output_gain,
    output_matrix,
):
    tp_count = lax.axis_size("tp")
    tp_index = lax.axis_index("tp")
    per_head = max(tp_count // HEADS, 1)
    heads_per_shard = max(HEADS // tp_count, 1)
    leading_head = tp_index // per_head * heads_per_shard
    tok_rows = latent.shape[0]
    conds = jax.nn.silu(
        jnp.stack([conditioning, context_prompt_vector]).astype(jnp.float32)
    ).astype(jnp.bfloat16)
    shifts, scales, gates = lax.psum(
        (
            linear(conds, shift_matrix),
            linear(conds, scale_matrix),
            linear(conds, residual_gate_matrix),
        ),
        "sp",
    )
    down_both = jnp.concatenate([decay_down_factor[0].T, decay_down_factor[1].T], axis=0)
    lat_weights = (query_matrix, key_matrix, value_matrix, gate_matrix, down_both)
    ctx_weights = (key_matrix, value_matrix, down_both)
    lat_f = latent.astype(jnp.float32)
    ctx_f = context.astype(jnp.float32)
    lat_sum, lat_squares, ctx_sum, ctx_squares = lax.psum(
        (
            jnp.sum(lat_f, axis=1, keepdims=True),
            jnp.sum(lat_f * lat_f, axis=1, keepdims=True),
            jnp.sum(ctx_f, axis=1, keepdims=True),
            jnp.sum(ctx_f * ctx_f, axis=1, keepdims=True),
        ),
        "tp",
    )
    latent_normalized = modulated(latent, lat_sum, lat_squares, shifts[0], scales[0])
    normed_ctx = modulated(context, ctx_sum, ctx_squares, shifts[1], scales[1])
    lat_piece = lax.all_gather(latent_normalized, "tp", axis=1, tiled=True)
    ctx_piece = lax.all_gather(normed_ctx, "tp", axis=1, tiled=True)
    lat_new = tuple((linear(lat_piece, weight) for weight in lat_weights))
    ctx_new = tuple((linear(ctx_piece, weight) for weight in ctx_weights))
    query_part, key_part, value_part, gate_part, low_rank_part = lat_new
    ctx_key_part, ctx_value_part, ctx_low = ctx_new
    query_full, key_full, ctx_key_full = head_channels(
        (stored(query_part), stored(key_part), stored(ctx_key_part)), per_head, tp_index
    )

    def split_heads(rows, width):
        return rows.astype(jnp.float32).reshape(rows.shape[0], heads_per_shard, width)

    value_cols = value_part.shape[1] // heads_per_shard
    queries = split_heads(query_full, DK) * DK ** (-0.5)
    key_rows = split_heads(key_full, DK)
    ctx_keys = split_heads(ctx_key_full, DK)
    values_lat = split_heads(stored(value_part), value_cols)
    values_ctx = split_heads(stored(ctx_value_part), value_cols)
    gate_rows = stored(gate_part).astype(jnp.float32)

    def per_head_decay(low_rows, direction):
        up_part = lax.dynamic_slice_in_dim(
            decay_up_factor[direction], leading_head * DK, heads_per_shard * DK, 1
        ).astype(jnp.float32)
        bias_part = lax.dynamic_slice_in_dim(
            decay_key_bias[direction], leading_head * DK, heads_per_shard * DK, 0
        )
        pre_act = jnp.dot(low_rows, up_part, precision=precise) + bias_part
        return (jax.nn.log_sigmoid(pre_act) / gate_norm).reshape(
            low_rows.shape[0], heads_per_shard, DK
        )

    decay_spikes = lax.dynamic_slice_in_dim(spike_log_decay, leading_head, heads_per_shard, 2)
    latent_forward = per_head_decay(low_rank_part[:, :DECAY_RANK], 0) + decay_spikes[0][:, :, None]
    latent_backward = per_head_decay(low_rank_part[:, DECAY_RANK:], 1) + decay_spikes[1][:, :, None]
    ctx_fwd = per_head_decay(ctx_low[:, :DECAY_RANK], 0)
    ctx_bwd = per_head_decay(ctx_low[:, DECAY_RANK:], 1)
    cf_growth, cf_state = end_state(ctx_keys, values_ctx, ctx_fwd)
    cb_growth, cb_state = end_state(
        reverse_rows(ctx_keys), reverse_rows(values_ctx), reverse_rows(ctx_bwd)
    )
    lf_growth, lf_state = end_state(key_rows, values_lat, latent_forward)
    lb_growth, lb_state = end_state(
        reverse_rows(key_rows), reverse_rows(values_lat), reverse_rows(latent_backward)
    )
    identity = (
        jnp.ones((heads_per_shard, DK), jnp.float32),
        jnp.zeros((heads_per_shard, DK, value_cols), jnp.float32),
    )
    ctx_gathered = (
        lax.all_gather(cf_growth[None].astype(jnp.bfloat16), "sp", axis=0, tiled=True).astype(
            jnp.float32
        ),
        lax.all_gather(cf_state[None].astype(jnp.bfloat16), "sp", axis=0, tiled=True).astype(
            jnp.float32
        ),
        lax.all_gather(cb_growth[None].astype(jnp.bfloat16), "sp", axis=0, tiled=True).astype(
            jnp.float32
        ),
        lax.all_gather(cb_state[None].astype(jnp.bfloat16), "sp", axis=0, tiled=True).astype(
            jnp.float32
        ),
    )
    total_fwd, total_bwd = context_totals(
        ctx_gathered[0], ctx_gathered[1], ctx_gathered[2], ctx_gathered[3], identity
    )
    prefix = carried_in((lf_growth, lf_state), "sp", combine, identity, False)
    suffix = carried_in((lb_growth, lb_state), "sp", combine, identity, True)
    start_fwd = combine(total_fwd, prefix)[1]
    start_bwd = combine(total_bwd, suffix)[1]
    zero_state = jnp.zeros((heads_per_shard, DK, value_cols), jnp.float32)

    def direction_out(query_rows, key_list, value_list, log_decay, start_state):
        local_part = blockwise(query_rows, key_list, value_list, log_decay, zero_state, BLK)
        reach = query_rows * jnp.exp(jnp.cumsum(log_decay, axis=0))
        return local_part + jnp.einsum("nhd,hde->nhe", reach, start_state, precision=precise)

    out_fwd = direction_out(queries, key_rows, values_lat, latent_forward, start_fwd)
    out_bwd = reverse_rows(
        direction_out(
            reverse_rows(queries),
            reverse_rows(key_rows),
            reverse_rows(values_lat),
            reverse_rows(latent_backward),
            start_bwd,
        )
    )
    grouped = (out_fwd + out_bwd).reshape(tok_rows, -1, VGROUP)
    grouped = grouped * lax.rsqrt(jnp.mean(grouped * grouped, axis=-1, keepdims=True) + epsilon)
    heads_out = (grouped.reshape(tok_rows, -1) * output_gain * jax.nn.silu(gate_rows)).astype(
        jnp.bfloat16
    )
    branch = linear(lax.all_gather(heads_out, "tp", axis=1, tiled=True), output_matrix)
    return (latent.astype(jnp.float32) + gates[0] * branch).astype(jnp.bfloat16)


def solution(mesh):
    placed = (
        P("sp", "tp"),
        P("sp", "tp"),
        P("sp"),
        P("sp"),
        P("tp", "sp"),
        P("tp", "sp"),
        P("tp", "sp"),
        P("tp", None),
        P("tp", None),
        P("tp", None),
        P("tp", None),
        P(),
        P(),
        P(),
        P(None, "sp", None),
        P("tp"),
        P("tp", None),
    )
    return jax.shard_map(
        local, mesh=mesh, in_specs=placed, out_specs=P("sp", "tp"), check_vma=False
    )
```

profile of v0, /device:TPU:0, one launch (start us, length us, event | category | flops | bytes accessed | tf_op | source)
XLA Modules:
  0.0 266.8 jit_solution(12194387579442730119)
XLA Ops:
  6.5 0.9 stack.10
  8.1 1.6 fusion.121
  9.7 1.6 fusion.123
  11.3 1.6 fusion.125
  12.9 1.0 convert_reduce_fusion
  14.8 13.2 %all-reduce.1 = (f32[2,512]{1,0:T(2,128)S(1)}, f32[2,512]{1,0:T(2,128)S(1)}, f32[2,512]{1,0:T(2,128)}) all-reduce(f32[2,512]{1,0:T(2,128)S(1)} %fusion.121, f32[2,512]{1,0:T(2,128)S(1)} %fusion.123, f32[2,512]{1,0:T(2,128)S(1)} %fusion.125), channel_id=1, replica_groups=mesh['sp'=4,'tp'=8] {'sp'}, use_global_device_ids=true, to_apply=%region_6.7 | all-reduce | flops 3072 | bytes 24576 | tf_op jit(solution)/shard_map/psum | solution.py:178
  28.0 21.7 %all-reduce = (f32[128,1]{0,1:T(1,128)S(1)}, f32[128,1]{0,1:T(1,128)S(1)}, f32[16,1]{0,1:T(1,128)S(1)}, f32[16,1]{0,1:T(1,128)S(1)}) all-reduce(f32[128,1]{0,1:T(1,128)S(1)} %bitcast.291, f32[128,1]{0,1:T(1,128)S(1)} %bitcast.290, f32[16,1]{0,1:T(1,128)S(1)} %bitcast.293, f32[16,1]{0,1:T(1,128)S(1)} %bitcast.292), channel_id=1, replica_groups=mesh['sp'=4,'tp'=8] {'tp'}, use_global_device_ids=true, to_apply=%region_4.5 | all-reduce | flops 288 | bytes 2304 | tf_op jit(solution)/shard_map/psum | solution.py:191
  49.7 1.7 fusion.62
  52.3 1.0 slice_bitcast_fusion.3
  53.5 31.0 %all_gather.45 = bf16[16,4096]{1,0:T(8,128)(2,1)S(1)} all-gather(bf16[16,512]{1,0:T(8,128)(2,1)S(1)} %fusion.89), channel_id=1, replica_groups=mesh['sp'=4,'tp'=8] {'tp'}, dimensions={1}, use_global_device_ids=true | all-gather | bytes 147456 | tf_op jit(solution)/shard_map/all_gather | solution.py:203
  84.9 3.4 %convolution_convert_fusion.8 = bf16[16,512]{1,0:T(8,128)(2,1)S(1)} fusion(bf16[16,4096]{1,0:T(8,128)(2,1)S(1)} %all_gather.45, bf16[512,4096]{1,0:T(8,128)(2,1)} %param.38), kind=kOutput, calls=%fused_computation.96 | convolution fusion | flops 67117056 | bytes 4341760 | tf_op jit(solution)/shard_map/dot_general | solution.py:54
  89.8 5.1 %all_gather.46 = bf16[4,2,128]{2,1,0:T(2,128)(2,1)S(1)} all-gather(bf16[1,2,128]{2,1,0:T(2,128)(2,1)S(1)} %get-tuple-element.728), channel_id=1, replica_groups=mesh['sp'=4,'tp'=8] {'sp'}, dimensions={0}, use_global_device_ids=true | all-gather | bytes 2560 | tf_op jit(solution)/shard_map/all_gather | solution.py:253
  95.8 7.3 %all-gather.1 = bf16[8,128,256]{2,1,0:T(8,128)(2,1)S(1)} all-gather(bf16[2,128,256]{2,1,0:T(8,128)(2,1)S(1)} %convolution_convert_fusion.5), channel_id=3, replica_groups=mesh['sp'=4,'tp'=8] {'sp'}, dimensions={0}, use_global_device_ids=true | all-gather | bytes 655360 | tf_op jit(solution)/shard_map/all_gather | solution.py:256
  106.9 5.0 %all_gather.51 = bf16[4,2,128]{2,1,0:T(2,128)(2,1)S(1)} all-gather(bf16[1,2,128]{2,1,0:T(2,128)(2,1)S(1)} %get-tuple-element.734), channel_id=1, replica_groups=mesh['sp'=4,'tp'=8] {'sp'}, dimensions={0}, use_global_device_ids=true | all-gather | bytes 2560 | tf_op jit(solution)/shard_map/all_gather | solution.py:259
  112.7 1.1 convolution_convert_fusion.4
  113.8 7.5 %all-gather.3 = bf16[8,128,256]{2,1,0:T(8,128)(2,1)S(1)} all-gather(bf16[2,128,256]{2,1,0:T(8,128)(2,1)S(1)} %convolution_convert_fusion.4), channel_id=5, replica_groups=mesh['sp'=4,'tp'=8] {'sp'}, dimensions={0}, use_global_device_ids=true | all-gather | bytes 655360 | tf_op jit(solution)/shard_map/all_gather | solution.py:262
  121.3 1.1 convert.9
  122.4 4.4 %while.91 = (s32[]{:T(128)}, f32[2,128,256]{2,1,0:T(8,128)S(1)}, f32[4,2,128]{2,1,0:T(2,128)S(1)}, f32[4,2,128,256]{3,2,1,0:T(8,128)}, s32[]{:T(128)}, /*index=5*/s32[]{:T(128)}, s32[]{:T(128)}) while((s32[]{:T(128)}, f32[2,128,256]{2,1,0:T(8,128)S(1)}, f32[4,2,128]{2,1,0:T(2,128)S(1)}, f32[4,2,128,256]{3,2,1,0:T(8,128)}, ...), condition=%wide.region_28.29_spmd.clone, body=%wide.region_27.28_spmd.clone.sunk | while | flops 196612 | bytes 789619 | solution.py:142
  122.4 1.1 bitcast_add_fusion.5
  123.5 1.1 bitcast_add_fusion.5
  124.6 1.1 bitcast_add_fusion.5
  125.7 1.1 bitcast_add_fusion.5
  127.5 1.8 fusion.70
  129.3 1.7 fusion.74
  131.0 1.0 fusion.72
  133.5 2.1 convolution_convert_fusion.7
  137.0 3.7 %convolution_convert_fusion.2 = bf16[128,512]{1,0:T(8,128)(2,1)S(1)} fusion(bf16[128,4096]{1,0:T(8,128)(2,1)S(1)} %copy-done.1, bf16[512,4096]{1,0:T(8,128)(2,1)} %param.38), kind=kOutput, calls=%fused_computation.85 | convolution fusion | flops 536936448 | bytes 5373952 | tf_op jit(solution)/shard_map/dot_general | solution.py:54
  142.3 3.1 %convolution_convert_fusion.6 = bf16[128,256]{1,0:T(8,128)(2,1)} fusion(bf16[128,4096]{1,0:T(8,128)(2,1)S(1)} %copy-done.1, bf16[256,4096]{1,0:T(8,128)(2,1)} %param.36), kind=kOutput, calls=%fused_computation.94 | convolution fusion | flops 268468224 | bytes 3211264 | tf_op jit(solution)/shard_map/dot_general | solution.py:54
  145.4 1.6 reshape.143
  146.9 1.5 broadcast_multiply_fusion
  148.4 4.4 %convolution_convert_fusion = bf16[128,512]{1,0:T(8,128)(2,1)} fusion(bf16[128,4096]{1,0:T(8,128)(2,1)S(1)} %copy-done.1, bf16[512,4096]{1,0:T(8,128)(2,1)} %param.39), kind=kOutput, calls=%fused_computation.83 | convolution fusion | flops 536936448 | bytes 5373952 | tf_op jit(solution)/shard_map/dot_general | solution.py:54
  152.8 1.0 reshape.144
  153.8 1.0 broadcast_add_fusion
  154.9 1.0 rev.32
  155.9 1.0 copy.163
  157.7 1.1 fusion.83
  158.9 2.3 exponential_multiply_fusion.2
  161.9 5.9 %while.89 = (s32[]{:T(128)}, f32[2,128,256]{2,1,0:T(8,128)S(1)}, f32[2,64,2,256]{3,1,0,2:T(8,128)}, f32[2,64,2,128]{3,2,1,0:T(2,128)S(1)}, f32[2,64,2,128]{3,2,1...) while((s32[]{:T(128)}, f32[2,128,256]{2,1,0:T(8,128)S(1)}, ...), condition=%wide.region_22.23_spmd.clone, body=%wide.region_20.22_spmd.clone.sunk | while | flops 139837440 | bytes 2366588 | solution.py:109
  162.0 1.0 bitcast_multiply_fusion.9
  163.9 0.9 fusion.210
  164.9 1.0 bitcast_multiply_fusion.9
  166.9 0.9 fusion.210
  167.8 1.9 copy.96
  169.7 5.1 %all_gather.48 = bf16[4,2,128]{2,1,0:T(2,128)(2,1)S(1)} all-gather(bf16[1,2,128]{2,1,0:T(2,128)(2,1)} %get-tuple-element.724), channel_id=1, replica_groups=mesh['sp'=4,'tp'=8] {'sp'}, dimensions={0}, use_global_device_ids=true | all-gather | bytes 2560 | tf_op jit(solution)/shard_map/all_gather | solution.py:32
  174.8 1.3 convolution_convert_fusion.1
  176.1 7.9 %all-gather.2 = bf16[8,128,256]{2,1,0:T(8,128)(2,1)} all-gather(bf16[2,128,256]{2,1,0:T(8,128)(2,1)S(1)} %convolution_convert_fusion.1), channel_id=4, replica_groups=mesh['sp'=4,'tp'=8] {'sp'}, dimensions={0}, use_global_device_ids=true | all-gather | bytes 655360 | tf_op jit(solution)/shard_map/all_gather | solution.py:32
  184.0 4.4 %while.90 = (s32[]{:T(128)}, f32[2,128]{1,0:T(2,128)S(1)}, f32[2,128,256]{2,1,0:T(8,128)S(1)}, s32[]{:T(128)}, bf16[4,2,128]{2,1,0:T(2,128)(2,1)S(1)}, /*index=5...) while((s32[]{:T(128)}, f32[2,128]{1,0:T(2,128)S(1)}, ...), condition=%wide.region_25.26_spmd.clone, body=%wide.region_24.25_spmd.clone.sunk | while | flops 328968 | bytes 660669 | solution.py:50
  184.0 1.0 fusion.211
  185.1 1.0 fusion.211
  186.2 1.0 fusion.211
  187.3 1.0 fusion.211
  188.4 2.4 fusion.46
  190.8 3.1 %rev.38 = f32[128,2,256]{0,2,1:T(8,128)} reverse(f32[128,2,256]{0,2,1:T(8,128)} %fusion.46), dimensions={0} | reverse | bytes 524288 | tf_op jit(solution)/shard_map/jit(_flip)/rev | solution.py:69
  194.0 1.1 broadcast_add_fusion.1
  195.8 4.3 %while.86 = (s32[]{:T(128)}, f32[2,128,256]{2,1,0:T(8,128)S(1)}, f32[2,64,2,256]{3,1,0,2:T(8,128)}, f32[2,64,2,128]{3,2,1,0:T(2,128)S(1)}, f32[2,64,2,128]{3,2,1...) while((s32[]{:T(128)}, f32[2,128,256]{2,1,0:T(8,128)S(1)}, ...), condition=%wide.region_9.10_spmd.clone, body=%wide.region_7.9_spmd.clone.sunk | while | flops 139837440 | bytes 2594944 | solution.py:109
  197.1 0.9 fusion.196
  199.2 0.9 fusion.196
  200.1 1.8 copy.86
  201.9 5.0 %all_gather.42 = bf16[4,2,128]{2,1,0:T(2,128)(2,1)S(1)} all-gather(bf16[1,2,128]{2,1,0:T(2,128)(2,1)S(1)} %get-tuple-element.720), channel_id=1, replica_groups=mesh['sp'=4,'tp'=8] {'sp'}, dimensions={0}, use_global_device_ids=true | all-gather | bytes 2560 | tf_op jit(solution)/shard_map/all_gather | solution.py:32
  207.3 7.6 %all-gather = bf16[8,128,256]{2,1,0:T(8,128)(2,1)S(1)} all-gather(bf16[2,128,256]{2,1,0:T(8,128)(2,1)S(1)} %convolution_convert_fusion.3), channel_id=2, replica_groups=mesh['sp'=4,'tp'=8] {'sp'}, dimensions={0}, use_global_device_ids=true | all-gather | bytes 655360 | tf_op jit(solution)/shard_map/all_gather | solution.py:32
  215.7 1.7 fusion.130
  217.8 1.7 fusion.68
  219.5 35.8 %all-gather.9.cloned.1.call-done = bf16[128,4096]{1,0:T(8,128)(2,1)} async-done(((bf16[128,512]{1,0:T(8,128)(2,1)}), bf16[128,4096]{1,0:T(8,128)(2,1)}) %all-gather.9.cloned.1.call-update) | async-done | bytes 1048592 | tf_op jit(solution)/shard_map/all_gather | solution.py:295
  255.3 4.7 %fusion.50 = bf16[128,512]{1,0:T(8,128)(2,1)} fusion(bf16[128,4096]{1,0:T(8,128)(2,1)} %all-gather.9.cloned.1.call-done, bf16[512,4096]{1,0:T(8,128)(2,1)} %param.45, bf16[128,512]{1,0:T(8,128)(2,1)S(1)} %copy-done.11, f32[512]{0:T(512)S(1)} %bitcast.285), kind=kOutput, calls=%fused_computation.87 | convolution fusion | flops 537133056 | bytes 5507072 | tf_op jit(solution)/shard_map/dot_general | solution.py:54
  (178 shorter events, 24.6 us)
Async XLA Ops:
  6.5 82.4 %copy-start = (bf16[256,4096]{1,0:T(8,128)(2,1)S(1)}, bf16[256,4096]{1,0:T(8,128)(2,1)}, u32[]{:S(2)}) copy-start(bf16[256,4096]{1,0:T(8,128)(2,1)} %param.37) | copy-start | bytes 6291460
  6.5 46.8 %copy-start.17 = (bf16[16,512]{1,0:T(8,128)(2,1)S(1)}, bf16[16,512]{1,0:T(8,128)(2,1)}, u32[]{:S(2)}) copy-start(bf16[16,512]{1,0:T(8,128)(2,1)} %param.30) | copy-start | bytes 49156
  6.5 46.7 %copy-start.16 = (bf16[2,16,2048]{2,1,0:T(8,128)(2,1)S(1)}, bf16[2,16,2048]{2,1,0:T(8,128)(2,1)}, u32[]{:S(2)}) copy-start(bf16[2,16,2048]{2,1,0:T(8,128)(2,1)} %param.41) | copy-start | bytes 393220
  6.5 121.0 %all-gather.7.cloned.1.call-start = ((), (), s32[]{:S(2)}) async-start(), calls=%async_computation | async-start | bytes 1179648 | tf_op jit(solution)/shard_map/all_gather | solution.py:202
  51.4 203.9 %all-gather.9.cloned.1.call-start = ((), (), s32[]{:S(2)}) async-start(), calls=%async_computation.1 | async-start | bytes 1179648 | tf_op jit(solution)/shard_map/all_gather | solution.py:295
  53.3 49.8 %copy-start.15 = (bf16[16,4096]{1,0:T(8,128)(2,1)}, bf16[16,4096]{1,0:T(8,128)(2,1)S(1)}, u32[]{:S(2)}) copy-start(bf16[16,4096]{1,0:T(8,128)(2,1)S(1)} %get-tuple-element.713) | copy-start | bytes 393220
  53.3 49.8 %copy-start.18 = (bf16[1,16,2048]{2,1,0:T(8,128)(2,1)}, bf16[1,16,2048]{2,1,0:T(8,128)(2,1)S(1)}, u32[]{:S(2)}) copy-start(bf16[1,16,2048]{2,1,0:T(8,128)(2,1)S(1)} %get-tuple-element.721) | copy-start | bytes 196612
  53.3 49.8 %copy-start.19 = (bf16[1,16,2048]{2,1,0:T(8,128)(2,1)}, bf16[1,16,2048]{2,1,0:T(8,128)(2,1)S(1)}, u32[]{:S(2)}) copy-start(bf16[1,16,2048]{2,1,0:T(8,128)(2,1)S(1)} %get-tuple-element.722) | copy-start | bytes 196612
  84.4 5.4 %copy-start.22 = (f32[1,256]{1,0:T(1,128)}, f32[1,256]{1,0:T(1,128)S(1)}, u32[]{:S(2)}) copy-start(f32[1,256]{1,0:T(1,128)S(1)} %get-tuple-element.747) | copy-start | bytes 3076
  103.9 0.8 copy-start.3
  126.8 0.7 copy-start.5
  127.5 9.4 %copy-start.1 = (bf16[128,4096]{1,0:T(8,128)(2,1)S(1)}, bf16[128,4096]{1,0:T(8,128)(2,1)}, u32[]{:S(2)}) copy-start(bf16[128,4096]{1,0:T(8,128)(2,1)} %all-gather.7.cloned.1.call-done) | copy-start | bytes 3145732
  152.8 9.1 %copy-start.2 = (f32[2,128,256]{2,1,0:T(8,128)S(1)}, f32[2,128,256]{2,1,0:T(8,128)}, u32[]{:S(2)}) copy-start(f32[2,128,256]{2,1,0:T(8,128)} %custom-call.4) | copy-start | bytes 786436
  161.9 22.1 %copy-start.8 = (f32[2,128,256]{2,1,0:T(8,128)S(1)}, f32[2,128,256]{2,1,0:T(8,128)}, u32[]{:S(2)}) copy-start(f32[2,128,256]{2,1,0:T(8,128)} %custom-call.6) | copy-start | bytes 786436
  167.8 20.6 %copy-start.6 = (f32[2,128,256]{2,1,0:T(8,128)S(1)}, f32[2,128,256]{2,1,0:T(8,128)}, u32[]{:S(2)}) copy-start(f32[2,128,256]{2,1,0:T(8,128)} %copy-done.5) | copy-start | bytes 786436
  167.8 28.0 %copy-start.9 = (f32[2,64,2,256]{3,2,1,0:T(2,128)S(1)}, f32[2,64,2,256]{3,2,1,0:T(2,128)}, u32[]{:S(2)}) copy-start(f32[2,64,2,256]{3,2,1,0:T(2,128)} %reshape_reshape.7) | copy-start | bytes 786436
  176.1 17.8 %copy-start.14 = (f32[128,256]{1,0:T(8,128)S(1)}, f32[128,256]{1,0:T(8,128)}, u32[]{:S(2)}) copy-start(f32[128,256]{1,0:T(8,128)} %broadcast_multiply_fusion) | copy-start | bytes 393220
  176.1 19.7 %copy-start.10 = (f32[2,64,2,128]{3,2,1,0:T(2,128)S(1)}, f32[2,64,2,128]{3,2,1,0:T(2,128)}, u32[]{:S(2)}) copy-start(f32[2,64,2,128]{3,2,1,0:T(2,128)} %reshape_reshape.6) | copy-start | bytes 393220
  195.8 11.2 %copy-start.13 = (f32[128,2,128]{2,1,0:T(2,128)S(1)}, f32[128,2,128]{2,1,0:T(2,128)}, u32[]{:S(2)}) copy-start(f32[128,2,128]{2,1,0:T(2,128)} %get-tuple-element.717) | copy-start | bytes 393220
  195.8 19.2 %copy-start.7 = (f32[2,128,256]{2,1,0:T(8,128)S(1)}, f32[2,128,256]{2,1,0:T(8,128)}, u32[]{:S(2)}) copy-start(f32[2,128,256]{2,1,0:T(8,128)} %custom-call.2) | copy-start | bytes 786436
  200.1 15.6 %copy-start.4 = (f32[2,128,256]{2,1,0:T(8,128)S(1)}, f32[2,128,256]{2,1,0:T(8,128)}, u32[]{:S(2)}) copy-start(f32[2,128,256]{2,1,0:T(8,128)} %copy-done.3) | copy-start | bytes 786436
  200.1 17.7 %copy-start.20 = (f32[512]{0:T(512)S(1)}, f32[512]{0:T(512)}, u32[]{:S(2)}) copy-start(f32[512]{0:T(512)} %param.44) | copy-start | bytes 6148
  207.3 8.4 %copy-start.12 = (f32[128,2,256]{0,2,1:T(8,128)S(1)}, f32[128,2,256]{0,2,1:T(8,128)}, u32[]{:S(2)}) copy-start(f32[128,2,256]{0,2,1:T(8,128)} %rev.38) | copy-start | bytes 786436
  207.3 12.2 %copy-start.21 = (f32[2,512]{1,0:T(2,128)S(1)}, f32[2,512]{1,0:T(2,128)}, u32[]{:S(2)}) copy-start(f32[2,512]{1,0:T(2,128)} %get-tuple-element.705) | copy-start | bytes 12292
  207.3 47.9 %copy-start.11 = (bf16[128,512]{1,0:T(8,128)(2,1)S(1)}, bf16[128,512]{1,0:T(8,128)(2,1)}, u32[]{:S(2)}) copy-start(bf16[128,512]{1,0:T(8,128)(2,1)} %param.29) | copy-start | bytes 393220
Sparse Core Ops, SparseCore 0:
  51.5 35.1 all-gather.6
  219.6 35.6 all-gather.8
where the time goes:
time: 269 us; the launch traced here: 267 us
  blocking collectives  116 us (43%)
  matrix products  46.5 us (17%)
  waiting for transfers between devices  35.8 us (13%)
  other arithmetic  28.5 us (11%)
  local copies, waits for them, and re-layouts  25 us (9%)
  between operations  13.9 us (5%)
    all_gather x1, waiting for transfers between devices, local(): lax.all_gather(heads_out, 'tp', axis=1, tiled=True)  35.8 us
    all_gather x1, blocking collectives, local(): ctx_piece = lax.all_gather(normed_ctx, 'tp', axis=1, tiled=True)  31 us
    dot_general x12, matrix products, linear(): lax.dot_general(rows, weight, (((1,), (1,)), ((), ())), preferred_element...  28.7 us
    all_gather x4, blocking collectives, carried_in(): lax.all_gather(part.astype(kind), axis)  25.6 us
    psum x1, blocking collectives, local(): lax.psum((jnp.sum(lat_f, axis=1, keepdims=True), jnp.sum(lat_f * lat_f, a...  21.7 us
    psum x1, blocking collectives, local(): lax.psum((linear(conds, shift_matrix), linear(conds, scale_matrix), linea...  13.2 us
    all_gather x1, blocking collectives, local(): lax.all_gather(cb_state[None].astype(jnp.bfloat16), 'sp', axis=0, tiled=T...  7.46 us
    all_gather x1, blocking collectives, local(): lax.all_gather(cf_state[None].astype(jnp.bfloat16), 'sp', axis=0, tiled=T...  7.28 us
  transfers between devices with their start and end apart: 2, of which 1 were waited for; matrix products, arithmetic and copies ran while one was open for 7% of the time, Pallas kernels for 0%

commit v1 on v0

--- a/solution.py
+++ b/solution.py
@@ -200,7 +200,12 @@
     latent_normalized = modulated(latent, lat_sum, lat_squares, shifts[0], scales[0])
     normed_ctx = modulated(context, ctx_sum, ctx_squares, shifts[1], scales[1])
     lat_piece = lax.all_gather(latent_normalized, "tp", axis=1, tiled=True)
-    ctx_piece = lax.all_gather(normed_ctx, "tp", axis=1, tiled=True)
+    ring = [normed_ctx]
+    for hop in range(7):
+        ring.append(lax.ppermute(ring[-1], "tp", [(dev, (dev + 1) % 8) for dev in range(8)]))
+    ctx_piece = jnp.roll(
+        jnp.concatenate(ring[::-1], axis=1), (lax.axis_index("tp") + 1) * ring[0].shape[1], axis=1
+    )
     lat_new = tuple((linear(lat_piece, weight) for weight in lat_weights))
     ctx_new = tuple((linear(ctx_piece, weight) for weight in ctx_weights))
     query_part, key_part, value_part, gate_part, low_rank_part = lat_new

time: 269 us -> 283 us (1.052)
  waiting for transfers between devices: 35.8 us -> 74.8 us
  blocking collectives: 116 us -> 85.5 us
  other arithmetic: 28.5 us -> 34 us
    ppermute x0 -> x7, waiting for transfers between devices: none -> 38.5 us  [local(): lax.ppermute(ring[-1], 'tp', [(dev, (dev + 1) % 8) for dev in range(8)])]
    all_gather x1 -> x0, blocking collectives: 31 us -> none  [local(): ctx_piece = lax.all_gather(normed_ctx, 'tp', axis=1, tiled=True)]
    add x8, other arithmetic: 4.77 us -> 8.55 us  [combine(): return (earlier[0] * later[0], later[0][..., None] * earlier[1] + later[1])]
  transfers between devices with their start and end apart: 2 -> 9, of which waited for: 1 -> 8; matrix products, arithmetic and copies ran while one was open for 7% -> 9% of each run, Pallas kernels for 0% -> 0%
where the time goes in v1:
time: 283 us; the launch traced here: 282 us
  blocking collectives  85.5 us (30%)
  waiting for transfers between devices  74.8 us (26%)
  matrix products  47.2 us (17%)
  other arithmetic  34 us (12%)
  local copies, waits for them, and re-layouts  25.2 us (9%)
  between operations  14 us (5%)
    ppermute x7, waiting for transfers between devices, local(): lax.ppermute(ring[-1], 'tp', [(dev, (dev + 1) % 8) for dev in range(8)])  38.5 us
    all_gather x1, waiting for transfers between devices, local(): lax.all_gather(heads_out, 'tp', axis=1, tiled=True)  36.3 us
    dot_general x12, matrix products, linear(): lax.dot_general(rows, weight, (((1,), (1,)), ((), ())), preferred_element...  28.7 us
    all_gather x4, blocking collectives, carried_in(): lax.all_gather(part.astype(kind), axis)  25.8 us
    psum x1, blocking collectives, local(): lax.psum((jnp.sum(lat_f, axis=1, keepdims=True), jnp.sum(lat_f * lat_f, a...  21.7 us
    psum x1, blocking collectives, local(): lax.psum((linear(conds, shift_matrix), linear(conds, scale_matrix), linea...  13.2 us
    add x8, other arithmetic, combine(): return (earlier[0] * later[0], later[0][..., None] * earlier[1] + later[1])  8.55 us
    all_gather x1, blocking collectives, local(): lax.all_gather(cb_state[None].astype(jnp.bfloat16), 'sp', axis=0, tiled=T...  7.46 us
  transfers between devices with their start and end apart: 9, of which 8 were waited for; matrix products, arithmetic and copies ran while one was open for 9% of the time, Pallas kernels for 0%

profile of v1, /device:TPU:0, one launch (start us, length us, event | category | flops | bytes accessed | tf_op | source)
XLA Modules:
  0.0 281.6 jit_solution(12522485515598361080)
XLA Ops:
  8.1 1.6 fusion.127
  9.7 1.6 fusion.129
  11.3 1.6 fusion.131
  12.9 1.0 convert_reduce_fusion
  14.8 13.2 %all-reduce.1 = (f32[2,512]{1,0:T(2,128)S(1)}, f32[2,512]{1,0:T(2,128)S(1)}, f32[2,512]{1,0:T(2,128)}) all-reduce(f32[2,512]{1,0:T(2,128)S(1)} %fusion.127, f32[2,512]{1,0:T(2,128)S(1)} %fusion.129, f32[2,512]{1,0:T(2,128)S(1)} %fusion.131), channel_id=1, replica_groups=mesh['sp'=4,'tp'=8] {'sp'}, use_global_device_ids=true, to_apply=%region_6.7 | all-reduce | flops 3072 | bytes 24576 | tf_op jit(solution)/shard_map/psum | solution.py:178
  28.0 21.7 %all-reduce = (f32[128,1]{0,1:T(1,128)S(1)}, f32[128,1]{0,1:T(1,128)S(1)}, f32[16,1]{0,1:T(1,128)S(1)}, f32[16,1]{0,1:T(1,128)S(1)}) all-reduce(f32[128,1]{0,1:T(1,128)S(1)} %bitcast.292, f32[128,1]{0,1:T(1,128)S(1)} %bitcast.291, f32[16,1]{0,1:T(1,128)S(1)} %bitcast.294, f32[16,1]{0,1:T(1,128)S(1)} %bitcast.293), channel_id=1, replica_groups=mesh['sp'=4,'tp'=8] {'tp'}, use_global_device_ids=true, to_apply=%region_4.5 | all-reduce | flops 288 | bytes 2304 | tf_op jit(solution)/shard_map/psum | solution.py:191
  51.1 6.4 %collective-permute-done = bf16[16,512]{1,0:T(8,128)(2,1)S(1)} collective-permute-done((bf16[16,512]{1,0:T(8,128)(2,1)S(1)}, bf16[16,512]{1,0:T(8,128)(2,1)S(1)}, u32[]{:S(2)}, u32[]{:S(2)}) %collective-permute-start) | collective-permute-done | bytes 16416 | tf_op jit(solution)/shard_map/ppermute | solution.py:205
  57.5 1.7 fusion.62
  59.3 4.7 %collective-permute-done.1 = bf16[16,512]{1,0:T(8,128)(2,1)S(1)} collective-permute-done((bf16[16,512]{1,0:T(8,128)(2,1)S(1)}, bf16[16,512]{1,0:T(8,128)(2,1)S(1)}, u32[]{:S(2)}, u32[]{:S(2)}) %collective-permute-start.1) | collective-permute-done | bytes 16416 | tf_op jit(solution)/shard_map/ppermute | solution.py:205
  64.9 5.4 %collective-permute-done.2 = bf16[16,512]{1,0:T(8,128)(2,1)S(1)} collective-permute-done((bf16[16,512]{1,0:T(8,128)(2,1)S(1)}, bf16[16,512]{1,0:T(8,128)(2,1)S(1)}, u32[]{:S(2)}, u32[]{:S(2)}) %collective-permute-start.2) | collective-permute-done | bytes 16416 | tf_op jit(solution)/shard_map/ppermute | solution.py:205
  71.0 5.8 %collective-permute-done.3 = bf16[16,512]{1,0:T(8,128)(2,1)S(1)} collective-permute-done((bf16[16,512]{1,0:T(8,128)(2,1)S(1)}, bf16[16,512]{1,0:T(8,128)(2,1)S(1)}, u32[]{:S(2)}, u32[]{:S(2)}) %collective-permute-start.3) | collective-permute-done | bytes 16416 | tf_op jit(solution)/shard_map/ppermute | solution.py:205
  76.9 6.4 %collective-permute-done.4 = bf16[16,512]{1,0:T(8,128)(2,1)S(1)} collective-permute-done((bf16[16,512]{1,0:T(8,128)(2,1)S(1)}, bf16[16,512]{1,0:T(8,128)(2,1)S(1)}, u32[]{:S(2)}, u32[]{:S(2)}) %collective-permute-start.4) | collective-permute-done | bytes 16416 | tf_op jit(solution)/shard_map/ppermute | solution.py:205
  83.9 6.0 %collective-permute-done.5 = bf16[16,512]{1,0:T(8,128)(2,1)S(1)} collective-permute-done((bf16[16,512]{1,0:T(8,128)(2,1)S(1)}, bf16[16,512]{1,0:T(8,128)(2,1)S(1)}, u32[]{:S(2)}, u32[]{:S(2)}) %collective-permute-start.5) | collective-permute-done | bytes 16416 | tf_op jit(solution)/shard_map/ppermute | solution.py:205
  92.9 3.7 %collective-permute-done.6 = bf16[16,512]{1,0:T(8,128)(2,1)S(1)} collective-permute-done((bf16[16,512]{1,0:T(8,128)(2,1)S(1)}, bf16[16,512]{1,0:T(8,128)(2,1)S(1)}, u32[]{:S(2)}, u32[]{:S(2)}) %collective-permute-start.6) | collective-permute-done | bytes 16416 | tf_op jit(solution)/shard_map/ppermute | solution.py:205
  99.3 3.4 %convolution_convert_fusion.8 = bf16[16,512]{1,0:T(8,128)(2,1)S(1)} fusion(bf16[512,4096]{1,0:T(8,128)(2,1)} %param.38, bf16[16,8192]{1,0:T(8,128)(2,1)S(1)} %constant_dynamic-update-slice_fusion, s32[]{:T(128)S(6)} %select_n.145), kind=kOutput, calls=%fused_computation.96 | convolution fusion | flops 67117056 | bytes 4341764 | tf_op jit(solution)/shard_map/dot_general | solution.py:54
  104.4 5.1 %all_gather.42 = bf16[4,2,128]{2,1,0:T(2,128)(2,1)S(1)} all-gather(bf16[1,2,128]{2,1,0:T(2,128)(2,1)S(1)} %get-tuple-element.728), channel_id=1, replica_groups=mesh['sp'=4,'tp'=8] {'sp'}, dimensions={0}, use_global_device_ids=true | all-gather | bytes 2560 | tf_op jit(solution)/shard_map/all_gather | solution.py:258
  109.8 7.3 %all-gather.1 = bf16[8,128,256]{2,1,0:T(8,128)(2,1)S(1)} all-gather(bf16[2,128,256]{2,1,0:T(8,128)(2,1)S(1)} %convolution_convert_fusion.5), channel_id=3, replica_groups=mesh['sp'=4,'tp'=8] {'sp'}, dimensions={0}, use_global_device_ids=true | all-gather | bytes 655360 | tf_op jit(solution)/shard_map/all_gather | solution.py:261
  117.1 1.0 convert.8
  118.1 4.4 %while.88 = (s32[]{:T(128)}, f32[2,128,256]{2,1,0:T(8,128)S(1)}, f32[4,2,128]{2,1,0:T(2,128)S(1)}, f32[4,2,128,256]{3,2,1,0:T(8,128)}, s32[]{:T(128)}, /*index=5*/s32[]{:T(128)}) while((s32[]{:T(128)}, f32[2,128,256]{2,1,0:T(8,128)S(1)}, f32[4,2,128]{2,1,0:T(2,128)S(1)}, f32[4,2,128,256]{3,2,1,0:T(8,128)}, s32[]{:T(128)}, ...), condition=%wide.region_19.20_spmd.clone, body=%wide.region_18.19_spmd.clone.sunk | while | flops 196611 | bytes 789599 | solution.py:141
  118.1 1.1 bitcast_add_fusion.4
  119.2 1.1 bitcast_add_fusion.4
  120.3 1.1 bitcast_add_fusion.4
  121.4 1.1 bitcast_add_fusion.4
  122.6 5.1 %all_gather.47 = bf16[4,2,128]{2,1,0:T(2,128)(2,1)S(1)} all-gather(bf16[1,2,128]{2,1,0:T(2,128)(2,1)S(1)} %get-tuple-element.734), channel_id=1, replica_groups=mesh['sp'=4,'tp'=8] {'sp'}, dimensions={0}, use_global_device_ids=true | all-gather | bytes 2560 | tf_op jit(solution)/shard_map/all_gather | solution.py:264
  128.1 7.5 %all-gather.3 = bf16[8,128,256]{2,1,0:T(8,128)(2,1)S(1)} all-gather(bf16[2,128,256]{2,1,0:T(8,128)(2,1)S(1)} %convolution_convert_fusion.4), channel_id=5, replica_groups=mesh['sp'=4,'tp'=8] {'sp'}, dimensions={0}, use_global_device_ids=true | all-gather | bytes 655360 | tf_op jit(solution)/shard_map/all_gather | solution.py:267
  135.6 1.0 convert.9
  136.6 4.4 %while.91 = (s32[]{:T(128)}, f32[2,128,256]{2,1,0:T(8,128)S(1)}, f32[4,2,128]{2,1,0:T(2,128)S(1)}, f32[4,2,128,256]{3,2,1,0:T(8,128)}, s32[]{:T(128)}, /*index=5*/s32[]{:T(128)}, s32[]{:T(128)}) while((s32[]{:T(128)}, f32[2,128,256]{2,1,0:T(8,128)S(1)}, f32[4,2,128]{2,1,0:T(2,128)S(1)}, f32[4,2,128,256]{3,2,1,0:T(8,128)}, ...), condition=%wide.region_28.29_spmd.clone, body=%wide.region_27.28_spmd.clone.sunk | while | flops 196612 | bytes 789619 | solution.py:142
  136.6 1.1 bitcast_add_fusion.5
  137.7 1.1 bitcast_add_fusion.5
  138.8 1.1 bitcast_add_fusion.5
  140.0 1.1 bitcast_add_fusion.5
  141.7 1.8 fusion.70
  143.5 1.7 fusion.74
  145.2 1.0 fusion.72
  147.7 2.1 convolution_convert_fusion.7
  151.2 3.7 %convolution_convert_fusion.2 = bf16[128,512]{1,0:T(8,128)(2,1)S(1)} fusion(bf16[128,4096]{1,0:T(8,128)(2,1)S(1)} %copy-done.1, bf16[512,4096]{1,0:T(8,128)(2,1)} %param.38), kind=kOutput, calls=%fused_computation.85 | convolution fusion | flops 536936448 | bytes 5373952 | tf_op jit(solution)/shard_map/dot_general | solution.py:54
  156.5 3.1 %convolution_convert_fusion.6 = bf16[128,256]{1,0:T(8,128)(2,1)} fusion(bf16[128,4096]{1,0:T(8,128)(2,1)S(1)} %copy-done.1, bf16[256,4096]{1,0:T(8,128)(2,1)} %param.36), kind=kOutput, calls=%fused_computation.94 | convolution fusion | flops 268468224 | bytes 3211264 | tf_op jit(solution)/shard_map/dot_general | solution.py:54
  159.6 1.6 reshape.143
  161.1 1.5 broadcast_multiply_fusion
  162.6 4.4 %convolution_convert_fusion = bf16[128,512]{1,0:T(8,128)(2,1)} fusion(bf16[128,4096]{1,0:T(8,128)(2,1)S(1)} %copy-done.1, bf16[512,4096]{1,0:T(8,128)(2,1)} %param.39), kind=kOutput, calls=%fused_computation.83 | convolution fusion | flops 536936448 | bytes 5373952 | tf_op jit(solution)/shard_map/dot_general | solution.py:54
  168.0 1.0 broadcast_add_fusion
  171.9 1.1 fusion.83
  173.0 2.3 exponential_multiply_fusion.2
  176.0 5.9 %while.89 = (s32[]{:T(128)}, f32[2,128,256]{2,1,0:T(8,128)S(1)}, f32[2,64,2,256]{3,1,0,2:T(8,128)}, f32[2,64,2,128]{3,2,1,0:T(2,128)S(1)}, f32[2,64,2,128]{3,2,1...) while((s32[]{:T(128)}, f32[2,128,256]{2,1,0:T(8,128)S(1)}, ...), condition=%wide.region_22.23_spmd.clone, body=%wide.region_20.22_spmd.clone.sunk | while | flops 139837440 | bytes 2366588 | solution.py:109
  182.0 1.8 copy.96
  183.8 5.3 %all_gather.44 = bf16[4,2,128]{2,1,0:T(2,128)(2,1)S(1)} all-gather(bf16[1,2,128]{2,1,0:T(2,128)(2,1)} %get-tuple-element.724), channel_id=1, replica_groups=mesh['sp'=4,'tp'=8] {'sp'}, dimensions={0}, use_global_device_ids=true | all-gather | bytes 2560 | tf_op jit(solution)/shard_map/all_gather | solution.py:32
  189.1 1.3 convolution_convert_fusion.1
  190.4 7.9 %all-gather.2 = bf16[8,128,256]{2,1,0:T(8,128)(2,1)} all-gather(bf16[2,128,256]{2,1,0:T(8,128)(2,1)S(1)} %convolution_convert_fusion.1), channel_id=4, replica_groups=mesh['sp'=4,'tp'=8] {'sp'}, dimensions={0}, use_global_device_ids=true | all-gather | bytes 655360 | tf_op jit(solution)/shard_map/all_gather | solution.py:32
  198.3 4.4 %while.90 = (s32[]{:T(128)}, f32[2,128]{1,0:T(2,128)S(1)}, f32[2,128,256]{2,1,0:T(8,128)S(1)}, s32[]{:T(128)}, bf16[4,2,128]{2,1,0:T(2,128)(2,1)S(1)}, /*index=5...) while((s32[]{:T(128)}, f32[2,128]{1,0:T(2,128)S(1)}, ...), condition=%wide.region_25.26_spmd.clone, body=%wide.region_24.25_spmd.clone.sunk | while | flops 328968 | bytes 660669 | solution.py:50
  198.3 1.0 fusion.214
  199.4 1.0 fusion.214
  200.5 1.0 fusion.214
  201.6 1.0 fusion.214
  202.7 2.4 fusion.46
  205.1 3.1 %rev.38 = f32[128,2,256]{0,2,1:T(8,128)} reverse(f32[128,2,256]{0,2,1:T(8,128)} %fusion.46), dimensions={0} | reverse | bytes 524288 | tf_op jit(solution)/shard_map/jit(_flip)/rev | solution.py:69
  208.2 1.1 broadcast_add_fusion.1
  210.1 4.3 %while.86 = (s32[]{:T(128)}, f32[2,128,256]{2,1,0:T(8,128)S(1)}, f32[2,64,2,256]{3,1,0,2:T(8,128)}, f32[2,64,2,128]{3,2,1,0:T(2,128)S(1)}, f32[2,64,2,128]{3,2,1...) while((s32[]{:T(128)}, f32[2,128,256]{2,1,0:T(8,128)S(1)}, ...), condition=%wide.region_9.10_spmd.clone, body=%wide.region_7.9_spmd.clone.sunk | while | flops 139837440 | bytes 2594944 | solution.py:109
  214.4 1.8 copy.86
  216.2 5.0 %all_gather.39 = bf16[4,2,128]{2,1,0:T(2,128)(2,1)S(1)} all-gather(bf16[1,2,128]{2,1,0:T(2,128)(2,1)S(1)} %get-tuple-element.720), channel_id=1, replica_groups=mesh['sp'=4,'tp'=8] {'sp'}, dimensions={0}, use_global_device_ids=true | all-gather | bytes 2560 | tf_op jit(solution)/shard_map/all_gather | solution.py:32
  221.6 7.6 %all-gather = bf16[8,128,256]{2,1,0:T(8,128)(2,1)S(1)} all-gather(bf16[2,128,256]{2,1,0:T(8,128)(2,1)S(1)} %convolution_convert_fusion.3), channel_id=2, replica_groups=mesh['sp'=4,'tp'=8] {'sp'}, dimensions={0}, use_global_device_ids=true | all-gather | bytes 655360 | tf_op jit(solution)/shard_map/all_gather | solution.py:32
  230.0 1.7 fusion.136
  232.0 1.7 fusion.68
  233.7 36.3 %all-gather.9.cloned.1.call-done = bf16[128,4096]{1,0:T(8,128)(2,1)} async-done(((bf16[128,512]{1,0:T(8,128)(2,1)}), bf16[128,4096]{1,0:T(8,128)(2,1)}) %all-gather.9.cloned.1.call-update) | async-done | bytes 1048592 | tf_op jit(solution)/shard_map/all_gather | solution.py:300
  270.0 4.7 %fusion.50 = bf16[128,512]{1,0:T(8,128)(2,1)} fusion(bf16[128,4096]{1,0:T(8,128)(2,1)} %all-gather.9.cloned.1.call-done, bf16[512,4096]{1,0:T(8,128)(2,1)} %param.45, bf16[128,512]{1,0:T(8,128)(2,1)S(1)} %copy-done.11, f32[512]{0:T(512)S(1)} %bitcast.288), kind=kOutput, calls=%fused_computation.87 | convolution fusion | flops 537133056 | bytes 5507072 | tf_op jit(solution)/shard_map/dot_general | solution.py:54
  (213 shorter events, 36.7 us)
Async XLA Ops:
  6.5 96.2 %copy-start = (bf16[256,4096]{1,0:T(8,128)(2,1)S(1)}, bf16[256,4096]{1,0:T(8,128)(2,1)}, u32[]{:S(2)}) copy-start(bf16[256,4096]{1,0:T(8,128)(2,1)} %param.37) | copy-start | bytes 6291460
  6.5 90.1 %copy-start.16 = (bf16[16,512]{1,0:T(8,128)(2,1)S(1)}, bf16[16,512]{1,0:T(8,128)(2,1)}, u32[]{:S(2)}) copy-start(bf16[16,512]{1,0:T(8,128)(2,1)} %param.30) | copy-start | bytes 49156
  6.5 63.8 %copy-start.17 = (bf16[2,16,2048]{2,1,0:T(8,128)(2,1)S(1)}, bf16[2,16,2048]{2,1,0:T(8,128)(2,1)}, u32[]{:S(2)}) copy-start(bf16[2,16,2048]{2,1,0:T(8,128)(2,1)} %param.41) | copy-start | bytes 393220
  6.5 70.3 %copy-start.18 = (f32[2,2048]{1,0:T(2,128)S(1)}, f32[2,2048]{1,0:T(2,128)}, u32[]{:S(2)}) copy-start(f32[2,2048]{1,0:T(2,128)} %param.42) | copy-start | bytes 49156
  6.5 135.2 %all-gather.7.cloned.1.call-start = ((), (), s32[]{:S(2)}) async-start(), calls=%async_computation | async-start | bytes 1179648 | tf_op jit(solution)/shard_map/all_gather | solution.py:202
  49.7 0.5 copy-start.19
  49.7 0.6 copy-start.20
  51.1 6.4 %collective-permute-start = (bf16[16,512]{1,0:T(8,128)(2,1)S(1)}, bf16[16,512]{1,0:T(8,128)(2,1)S(1)}, u32[]{:S(2)}, u32[]{:S(2)}) collective-permute-start(bf16[16,512]{1,0:T(8,128)(2,1)S(1)} %fusion.92), channel_id=1, source_target_pairs={{0,1},{1,2},{2,3},{3,4},{4,5},{5,6},{6,7},{7,0},{8,9},{9,10},{10,1... | collective-permute-start | bytes 49160 | tf_op jit(solution)/shard_map/ppermute | solution.py:205
  57.5 6.4 %collective-permute-start.1 = (bf16[16,512]{1,0:T(8,128)(2,1)S(1)}, bf16[16,512]{1,0:T(8,128)(2,1)S(1)}, u32[]{:S(2)}, u32[]{:S(2)}) collective-permute-start(bf16[16,512]{1,0:T(8,128)(2,1)S(1)} %collective-permute-done), channel_id=1, source_target_pairs={{0,1},{1,2},{2,3},{3,4},{4,5},{5,6},{6,7},{7,0},{8,9},{9,10},{10,1... | collective-permute-start | bytes 49160 | tf_op jit(solution)/shard_map/ppermute | solution.py:205
  59.2 210.8 %all-gather.9.cloned.1.call-start = ((), (), s32[]{:S(2)}) async-start(), calls=%async_computation.1 | async-start | bytes 1179648 | tf_op jit(solution)/shard_map/all_gather | solution.py:300
  63.9 6.4 %collective-permute-start.2 = (bf16[16,512]{1,0:T(8,128)(2,1)S(1)}, bf16[16,512]{1,0:T(8,128)(2,1)S(1)}, u32[]{:S(2)}, u32[]{:S(2)}) collective-permute-start(bf16[16,512]{1,0:T(8,128)(2,1)S(1)} %collective-permute-done.1), channel_id=1, source_target_pairs={{0,1},{1,2},{2,3},{3,4},{4,5},{5,6},{6,7},{7,0},{8,9},{9,10},{10,1... | collective-permute-start | bytes 49160 | tf_op jit(solution)/shard_map/ppermute | solution.py:205
  64.9 38.5 %copy-start.15 = (bf16[16,4096]{1,0:T(8,128)(2,1)}, bf16[16,4096]{1,0:T(8,128)(2,1)S(1)}, u32[]{:S(2)}) copy-start(bf16[16,4096]{1,0:T(8,128)(2,1)S(1)} %get-tuple-element.713) | copy-start | bytes 393220
  70.4 6.5 %collective-permute-start.3 = (bf16[16,512]{1,0:T(8,128)(2,1)S(1)}, bf16[16,512]{1,0:T(8,128)(2,1)S(1)}, u32[]{:S(2)}, u32[]{:S(2)}) collective-permute-start(bf16[16,512]{1,0:T(8,128)(2,1)S(1)} %collective-permute-done.2), channel_id=1, source_target_pairs={{0,1},{1,2},{2,3},{3,4},{4,5},{5,6},{6,7},{7,0},{8,9},{9,10},{10,1... | collective-permute-start | bytes 49160 | tf_op jit(solution)/shard_map/ppermute | solution.py:205
  76.8 6.4 %collective-permute-start.4 = (bf16[16,512]{1,0:T(8,128)(2,1)S(1)}, bf16[16,512]{1,0:T(8,128)(2,1)S(1)}, u32[]{:S(2)}, u32[]{:S(2)}) collective-permute-start(bf16[16,512]{1,0:T(8,128)(2,1)S(1)} %collective-permute-done.3), channel_id=1, source_target_pairs={{0,1},{1,2},{2,3},{3,4},{4,5},{5,6},{6,7},{7,0},{8,9},{9,10},{10,1... | collective-permute-start | bytes 49160 | tf_op jit(solution)/shard_map/ppermute | solution.py:205
  83.3 6.6 %collective-permute-start.5 = (bf16[16,512]{1,0:T(8,128)(2,1)S(1)}, bf16[16,512]{1,0:T(8,128)(2,1)S(1)}, u32[]{:S(2)}, u32[]{:S(2)}) collective-permute-start(bf16[16,512]{1,0:T(8,128)(2,1)S(1)} %collective-permute-done.4), channel_id=1, source_target_pairs={{0,1},{1,2},{2,3},{3,4},{4,5},{5,6},{6,7},{7,0},{8,9},{9,10},{10,1... | collective-permute-start | bytes 49160 | tf_op jit(solution)/shard_map/ppermute | solution.py:205
  89.9 6.6 %collective-permute-start.6 = (bf16[16,512]{1,0:T(8,128)(2,1)S(1)}, bf16[16,512]{1,0:T(8,128)(2,1)S(1)}, u32[]{:S(2)}, u32[]{:S(2)}) collective-permute-start(bf16[16,512]{1,0:T(8,128)(2,1)S(1)} %collective-permute-done.5), channel_id=1, source_target_pairs={{0,1},{1,2},{2,3},{3,4},{4,5},{5,6},{6,7},{7,0},{8,9},{9,10},{10,1... | collective-permute-start | bytes 49160 | tf_op jit(solution)/shard_map/ppermute | solution.py:205
  97.4 6.1 %copy-start.23 = (f32[1,256]{1,0:T(1,128)S(1)}, f32[1,256]{1,0:T(1,128)}, u32[]{:S(2)}) copy-start(f32[1,256]{1,0:T(1,128)} %get-tuple-element.748) | copy-start | bytes 3076
  122.5 18.5 %copy-start.5 = (f32[2,128,256]{2,1,0:T(8,128)}, f32[2,128,256]{2,1,0:T(8,128)S(1)}, u32[]{:S(2)}) copy-start(f32[2,128,256]{2,1,0:T(8,128)S(1)} %get-tuple-element.462) | copy-start | bytes 786436
  122.5 21.0 %copy-start.25 = (f32[1,256]{1,0:T(1,128)S(1)}, f32[1,256]{1,0:T(1,128)}, u32[]{:S(2)}) copy-start(f32[1,256]{1,0:T(1,128)} %get-tuple-element.747) | copy-start | bytes 3076
  122.5 22.7 %copy-start.24 = (f32[1,256]{1,0:T(1,128)S(1)}, f32[1,256]{1,0:T(1,128)}, u32[]{:S(2)}) copy-start(f32[1,256]{1,0:T(1,128)} %get-tuple-element.748) | copy-start | bytes 3076
  141.1 0.7 copy-start.3
  141.7 9.5 %copy-start.1 = (bf16[128,4096]{1,0:T(8,128)(2,1)S(1)}, bf16[128,4096]{1,0:T(8,128)(2,1)}, u32[]{:S(2)}) copy-start(bf16[128,4096]{1,0:T(8,128)(2,1)} %all-gather.7.cloned.1.call-done) | copy-start | bytes 3145732
  167.0 9.0 %copy-start.2 = (f32[2,128,256]{2,1,0:T(8,128)S(1)}, f32[2,128,256]{2,1,0:T(8,128)}, u32[]{:S(2)}) copy-start(f32[2,128,256]{2,1,0:T(8,128)} %custom-call.4) | copy-start | bytes 786436
  176.0 22.2 %copy-start.8 = (f32[2,128,256]{2,1,0:T(8,128)S(1)}, f32[2,128,256]{2,1,0:T(8,128)}, u32[]{:S(2)}) copy-start(f32[2,128,256]{2,1,0:T(8,128)} %custom-call.6) | copy-start | bytes 786436
  182.0 20.7 %copy-start.4 = (f32[2,128,256]{2,1,0:T(8,128)S(1)}, f32[2,128,256]{2,1,0:T(8,128)}, u32[]{:S(2)}) copy-start(f32[2,128,256]{2,1,0:T(8,128)} %copy-done.3) | copy-start | bytes 786436
  182.0 28.1 %copy-start.9 = (f32[2,64,2,256]{3,2,1,0:T(2,128)S(1)}, f32[2,64,2,256]{3,2,1,0:T(2,128)}, u32[]{:S(2)}) copy-start(f32[2,64,2,256]{3,2,1,0:T(2,128)} %reshape_reshape.7) | copy-start | bytes 786436
  190.4 17.8 %copy-start.14 = (f32[128,256]{1,0:T(8,128)S(1)}, f32[128,256]{1,0:T(8,128)}, u32[]{:S(2)}) copy-start(f32[128,256]{1,0:T(8,128)} %broadcast_multiply_fusion) | copy-start | bytes 393220
  190.4 19.7 %copy-start.10 = (f32[2,64,2,128]{3,2,1,0:T(2,128)S(1)}, f32[2,64,2,128]{3,2,1,0:T(2,128)}, u32[]{:S(2)}) copy-start(f32[2,64,2,128]{3,2,1,0:T(2,128)} %reshape_reshape.6) | copy-start | bytes 393220
  210.1 11.2 %copy-start.13 = (f32[128,2,128]{2,1,0:T(2,128)S(1)}, f32[128,2,128]{2,1,0:T(2,128)}, u32[]{:S(2)}) copy-start(f32[128,2,128]{2,1,0:T(2,128)} %get-tuple-element.717) | copy-start | bytes 393220
  210.1 19.1 %copy-start.7 = (f32[2,128,256]{2,1,0:T(8,128)S(1)}, f32[2,128,256]{2,1,0:T(8,128)}, u32[]{:S(2)}) copy-start(f32[2,128,256]{2,1,0:T(8,128)} %custom-call.2) | copy-start | bytes 786436
  214.3 15.6 %copy-start.6 = (f32[2,128,256]{2,1,0:T(8,128)S(1)}, f32[2,128,256]{2,1,0:T(8,128)}, u32[]{:S(2)}) copy-start(f32[2,128,256]{2,1,0:T(8,128)} %copy-done.5) | copy-start | bytes 786436
  214.4 17.7 %copy-start.21 = (f32[512]{0:T(512)S(1)}, f32[512]{0:T(512)}, u32[]{:S(2)}) copy-start(f32[512]{0:T(512)} %param.44) | copy-start | bytes 6148
  221.5 8.4 %copy-start.12 = (f32[128,2,256]{0,2,1:T(8,128)S(1)}, f32[128,2,256]{0,2,1:T(8,128)}, u32[]{:S(2)}) copy-start(f32[128,2,256]{0,2,1:T(8,128)} %rev.38) | copy-start | bytes 786436
  221.6 12.2 %copy-start.22 = (f32[2,512]{1,0:T(2,128)S(1)}, f32[2,512]{1,0:T(2,128)}, u32[]{:S(2)}) copy-start(f32[2,512]{1,0:T(2,128)} %get-tuple-element.705) | copy-start | bytes 12292
  221.6 48.4 %copy-start.11 = (bf16[128,512]{1,0:T(8,128)(2,1)S(1)}, bf16[128,512]{1,0:T(8,128)(2,1)}, u32[]{:S(2)}) copy-start(bf16[128,512]{1,0:T(8,128)(2,1)} %param.29) | copy-start | bytes 393220
Sparse Core Ops, SparseCore 0:
  59.3 40.6 all-gather.6
  233.8 36.1 all-gather.8
